TPU v7x, 32 devices: a whole 2x2x4 slice. The times are simulated.
32 devices in a mesh: grp: 2 (over y), kv: 4 (over z), tp: 4 (over x, core).
Axes of the slice: x: 2, y: 2, z: 4, core: 2. Of those that a mesh axis runs over, the one named last changes fastest.
Arguments:
- tokens: bfloat16 [128, 2048], P('grp', 'kv'), parts along dimension 0, may hold values from -64 to 64
- lengths: int32 [128], P(('grp', 'kv')), parts along dimension 0, may hold values from 1 to 4096, 32768 in all
- state: float32 [128, 8, 128, 256], P(('grp', 'kv'), 'tp'), parts along dimension 0, may hold values from -6 to 6
- key_block: bfloat16 [128, 8, 64, 128], P(('grp', 'kv'), 'tp'), parts along dimension 0, may hold values from -6 to 6
- value_block: bfloat16 [128, 8, 64, 256], P(('grp', 'kv'), 'tp'), parts along dimension 0, may hold values from -6 to 6
- cum_decay: float32 [128, 8, 64, 128], P(('grp', 'kv'), 'tp'), parts along dimension 0, as said below
- step_decay: float32 [128, 1024], P(('grp', 'kv'), 'tp'), parts along dimension 0
- g_mix: bfloat16 [2048], P('kv'), may hold values from 0.099609375 to 1.8984375
- w_query: bfloat16 [2048, 1024], P('kv', 'tp'), may hold values from -0.125 to 0.125
- w_key: bfloat16 [2048, 1024], P('kv', 'tp'), may hold values from -0.125 to 0.125
- w_value: bfloat16 [2048, 2048], P('kv', 'tp'), may hold values from -0.125 to 0.125
- w_outgate: bfloat16 [2048, 2048], P('kv', 'tp'), may hold values from -0.125 to 0.125
- w_decay: bfloat16 [2048, 1024], P('kv', 'tp'), may hold values from -0.5 to 0.5
- g_heads: bfloat16 [2048], P('tp'), may hold values from 0.099609375 to 1.8984375
- w_out: bfloat16 [2048, 2048], P('tp', 'kv'), may hold values from -0.125 to 0.125
- g_ffn: bfloat16 [2048], P('kv'), may hold values from 0.099609375 to 1.8984375
- w_gate: bfloat16 [2048, 5632], P('kv', 'tp'), may hold values from -0.125 to 0.125
- w_up: bfloat16 [2048, 5632], P('kv', 'tp'), may hold values from -0.125 to 0.125
- w_down: bfloat16 [5632, 2048], P('tp', 'kv'), may hold values from -0.078125 to 0.078125
Outputs:
- updated: bfloat16 [128, 2048], P('grp', 'kv'), parts along dimension 0
There are 2 independent parts, one for each index of `grp`. A program takes and returns all parts, laid end to end along the dimension named above; an argument that names none is the same for every part. Nothing has to cross between parts.
Inputs may be any that keep to these rules, and one draw needn't show every extreme that they name: `cum_decay`: along the block's positions the entries never rise.
All inputs are finite; a program needn't handle non-finite values. No bound on the sum of `lengths` on one device may be relied on, other than what follows from the above.
Results may differ from a plain program's by a relative error of at most 0.019.
Values may be sent and summed in bfloat16 or wider, within the bound.
A program may use at most 64 MiB of HBM per device.

v0:
```python
import functools

import jax
import jax.numpy as jnp
from jax import lax
from jax.experimental import pallas as pl
from jax.experimental.pallas import tpu as pltpu
from jax.sharding import PartitionSpec as P

f32 = jnp.float32
bf16 = jnp.bfloat16
epsilon = 1e-06
temper = 16.0
LANES = 128
MESH = pl.DeviceIdType.MESH


def silu(v):
    return v / (1.0 + jnp.exp(-v))


def far_first(n):
    return sorted(range(1, n), key=lambda o: (-min(o, n - o), -o))


def split_hi_lo(total):
    lane = lax.broadcasted_iota(jnp.int32, (total.shape[0], LANES), 1)
    wide = jnp.broadcast_to(total, (total.shape[0], LANES))
    high = wide.astype(bf16).astype(f32)
    return jnp.where(lane < LANES // 2, high, wide - high).astype(bf16)


def join_hi_lo(block):
    return block[:, :1] + block[:, LANES // 2 : LANES // 2 + 1]


def kernel(
    cfg,
    lengths,
    *refs,
):
    (n_kv, n_tp, names, bounds) = cfg
    count = len(names)
    hbm = dict(zip(names, refs[:count]))
    out_hbm = refs[count]
    rest = refs[count + 1 :]
    vm = dict(zip(names, rest[:count]))
    (
        out_vm,
        td_base,
        state_bf,
        q_ref,
        td_ref,
        qe_ref,
        head_ref,
        a_send,
        a_recv,
        b_send,
        b_recv,
        mixed_all,
        attn_all,
        gu_send,
        gu_recv,
        hid_all,
        down_all,
        local_sem,
        send_sem,
        recv_sem,
    ) = rest[count:]

    kv = lax.axis_index("kv")
    tp = lax.axis_index("tp")
    seqs, heads, dk, dv = vm["state"].shape
    block_len = vm["key_block"].shape[2]
    rows = vm["tokens"].shape[0]
    width = vm["tokens"].shape[1] * n_kv
    kw = heads * dk
    vw = heads * dv

    copies = {}
    for index, name in enumerate(names):
        copies[name] = pltpu.make_async_copy(hbm[name], vm[name], local_sem.at[index])
    for name in names[:EARLY]:
        copies[name].start()

    barrier = pltpu.get_barrier_semaphore()
    for o in range(1, n_kv):
        pl.semaphore_signal(
            barrier, inc=1, device_id={"kv": lax.rem(kv + o, n_kv)}, device_id_type=MESH
        )
    for o in range(1, n_tp):
        pl.semaphore_signal(
            barrier, inc=1, device_id={"tp": lax.rem(tp + o, n_tp)}, device_id_type=MESH
        )

    def gain(name):
        return vm[name][...].astype(f32).reshape(1, -1)

    sem_next = [0]

    def remote(src, dst, axis, target):
        index = sem_next[0]
        sem_next[0] += 1
        copy = pltpu.make_async_remote_copy(
            src_ref=src,
            dst_ref=dst,
            send_sem=send_sem.at[index],
            recv_sem=recv_sem.at[index],
            device_id={axis: target},
            device_id_type=MESH,
        )
        copy.start()
        return copy

    def scatter(send, recv):
        result = []
        for o in far_first(n_kv):
            target = lax.rem(kv + o, n_kv)
            result.append(remote(send.at[target], recv.at[o - 1], "kv", target))
        return result

    def gather(buffer, axis):
        me, n = (kv, n_kv) if axis == "kv" else (tp, n_tp)
        return [
            remote(buffer.at[me], buffer.at[me], axis, lax.rem(me + o, n)) for o in far_first(n)
        ]

    def wait_all(started):
        for copy in started:
            copy.wait()

    def store_rows(buffer, lo, value):
        for d in range(n_kv):
            buffer[d, :, lo : lo + value.shape[1]] = value[d * seqs : (d + 1) * seqs]

    def reduced(send, recv, lo, hi):
        total = send[kv, :, lo:hi].astype(f32)
        for o in range(n_kv - 1):
            total = total + recv[o, :, lo:hi].astype(f32)
        return total

    copies["tokens"].wait()
    copies["g_mix"].wait()
    inputs = vm["tokens"][...].astype(f32)
    scaled = (inputs * gain("g_mix")).astype(bf16)
    store_rows(a_send, 3 * kw, split_hi_lo(jnp.sum(inputs * inputs, axis=1, keepdims=True)))
    for index, name in enumerate(("w_query", "w_key", "w_decay")):
        copies[name].wait()
        part = jnp.dot(scaled, vm[name][...], preferred_element_type=f32)
        store_rows(a_send, index * kw, part.astype(bf16))
    for name in names[EARLY:]:
        copies[name].start()
    pl.semaphore_wait(barrier, n_kv - 1 + n_tp - 1)
    sent_a = scatter(a_send, a_recv)
    for index, name in enumerate(("w_value", "w_outgate")):
        copies[name].wait()
        part = jnp.dot(scaled, vm[name][...], preferred_element_type=f32)
        store_rows(b_send, index * vw, part.astype(bf16))
    sent_b = scatter(b_send, b_recv)

    copies["cum_decay"].wait()
    copies["state"].wait()
    ordinal = lax.broadcasted_iota(jnp.int32, (block_len, dk), 0)

    group = 8 if seqs % 8 == 0 else seqs

    def prepare(step, carry):
        base = pl.multiple_of(step * group, group)
        for h in range(heads):
            ends = []
            for sub in range(group):
                s = base + sub
                live = lax.rem(lengths[s], block_len)
                picked = jnp.where(ordinal == live - 1, vm["cum_decay"][s, h], 0.0)
                ends.append(jnp.sum(picked, axis=0, keepdims=True))
                state_bf[s, h] = vm["state"][s, h].astype(bf16)
            td_base[pl.ds(base, group), h * dk : (h + 1) * dk] = jnp.concatenate(ends, axis=0)
        return carry

    lax.fori_loop(0, seqs // group, prepare, 0)
    for name in ("step_decay", "key_block", "value_block", "g_heads"):
        copies[name].wait()

    wait_all(sent_a)
    inverse = lax.rsqrt(
        join_hi_lo(reduced(a_send, a_recv, 3 * kw, 3 * kw + LANES)) / width + epsilon
    )
    query = reduced(a_send, a_recv, 0, kw) * inverse * dk ** (-0.5)
    keys_new = reduced(a_send, a_recv, kw, 2 * kw) * inverse
    decay_pre = reduced(a_send, a_recv, 2 * kw, 3 * kw) * inverse
    log_sigmoid = jnp.minimum(decay_pre, 0.0) - jnp.log(1.0 + jnp.exp(-jnp.abs(decay_pre)))
    log_step = log_sigmoid / temper + vm["step_decay"][...]
    token_decay = td_base[...] + log_step
    q_ref[...] = query
    td_ref[...] = token_decay
    qe_ref[...] = query * jnp.exp(token_decay)

    live_ordinal = lax.broadcasted_iota(jnp.int32, (block_len, 1), 0)

    def attend(step, carry):
        base = pl.multiple_of(step * group, group)
        for h in range(heads):
            cols = slice(h * dk, (h + 1) * dk)
            qs = q_ref[pl.ds(base, group), cols]
            tds = td_ref[pl.ds(base, group), cols]
            qes = qe_ref[pl.ds(base, group), cols]
            outs = []
            for sub in range(group):
                s = base + sub
                live = lax.rem(lengths[s], block_len)
                left = jnp.broadcast_to(qes[sub : sub + 1], (16, dk)).astype(bf16)
                carried = jnp.dot(left, state_bf[s, h], preferred_element_type=f32)[:1]
                scores = jnp.sum(
                    qs[sub : sub + 1]
                    * vm["key_block"][s, h].astype(f32)
                    * jnp.exp(tds[sub : sub + 1] - vm["cum_decay"][s, h]),
                    axis=1,
                    keepdims=True,
                )
                scores = jnp.where(live_ordinal < live, scores, 0.0)
                in_block = jnp.sum(
                    scores * vm["value_block"][s, h].astype(f32), axis=0, keepdims=True
                )
                outs.append(carried + in_block)
            head_ref[pl.ds(base, group), h * dv : (h + 1) * dv] = jnp.concatenate(outs, axis=0)
        return carry

    lax.fori_loop(0, seqs // group, attend, 0)

    wait_all(sent_b)
    for h in range(heads):
        cols = slice(h * dv, (h + 1) * dv)
        keys = slice(h * dk, (h + 1) * dk)
        values_new = reduced(b_send, b_recv, h * dv, (h + 1) * dv) * inverse
        out_gate = reduced(b_send, b_recv, vw + h * dv, vw + (h + 1) * dv) * inverse
        own = jnp.sum(query[:, keys] * keys_new[:, keys], axis=1, keepdims=True)
        head_out = head_ref[:, cols] + own * values_new
        scale = lax.rsqrt(jnp.mean(head_out * head_out, axis=1, keepdims=True) + epsilon)
        normed = head_out * scale * gain("g_heads")[:, cols]
        mixed_all[kv, :, cols] = (normed * silu(out_gate)).astype(bf16)
    sent = gather(mixed_all, "kv")
    copies["w_out"].wait()
    wait_all(sent)

    mixed = mixed_all[...].reshape(rows, vw)
    attn_all[tp] = jnp.dot(mixed, vm["w_out"][...], preferred_element_type=f32).astype(bf16)
    sent = gather(attn_all, "tp")
    copies["g_ffn"].wait()
    copies["w_gate"].wait()
    copies["w_up"].wait()
    wait_all(sent)
    attention = attn_all[0].astype(f32)
    for t in range(1, n_tp):
        attention = attention + attn_all[t].astype(f32)
    middle = (inputs + attention).astype(bf16).astype(f32)
    normed_mid = (middle * gain("g_ffn")).astype(bf16)

    sent_gu = []
    for c, (lo, hi) in enumerate(bounds):
        if c == 0:
            square = jnp.sum(middle * middle, axis=1, keepdims=True)
            store_rows(gu_send[c], 2 * (hi - lo), split_hi_lo(square))
        for index, name in enumerate(("w_gate", "w_up")):
            part = jnp.dot(normed_mid, vm[name][:, lo:hi], preferred_element_type=f32)
            store_rows(gu_send[c], index * (hi - lo), part.astype(bf16))
        sent_gu.append(scatter(gu_send[c], gu_recv[c]))
    sent_hid = []
    mid_inverse = None
    for c, (lo, hi) in enumerate(bounds):
        w = hi - lo
        wait_all(sent_gu[c])
        if c == 0:
            total = join_hi_lo(reduced(gu_send[c], gu_recv[c], 2 * w, 2 * w + LANES))
            mid_inverse = lax.rsqrt(total / width + epsilon)
        gate = reduced(gu_send[c], gu_recv[c], 0, w) * mid_inverse
        up = reduced(gu_send[c], gu_recv[c], w, 2 * w) * mid_inverse
        hid_all[c][kv] = (silu(gate) * up).astype(bf16)
        sent_hid.append(gather(hid_all[c], "kv"))
    copies["w_down"].wait()
    down = None
    for c, (lo, hi) in enumerate(bounds):
        wait_all(sent_hid[c])
        hidden = hid_all[c][...].reshape(rows, hi - lo)
        part = jnp.dot(hidden, vm["w_down"][lo:hi], preferred_element_type=f32)
        down = part if down is None else down + part
    down_all[tp] = down.astype(bf16)
    wait_all(gather(down_all, "tp"))
    total = down_all[0].astype(f32)
    for t in range(1, n_tp):
        total = total + down_all[t].astype(f32)
    out_vm[...] = (middle + total).astype(bf16)
    result = pltpu.make_async_copy(out_vm, out_hbm, local_sem.at[count])
    result.start()
    result.wait()


ORDER = (
    "tokens",
    "g_mix",
    "w_query",
    "w_key",
    "w_decay",
    "w_value",
    "w_outgate",
    "cum_decay",
    "state",
    "step_decay",
    "key_block",
    "value_block",
    "g_heads",
    "w_out",
    "g_ffn",
    "w_gate",
    "w_up",
    "w_down",
)
CHUNKS = 2
EARLY = 7


def body(n_kv, n_tp, lengths, given):
    rows, columns = given["tokens"].shape
    seqs, heads, dk, dv = given["state"].shape
    kw, vw = heads * dk, heads * dv
    hidden = given["w_gate"].shape[1]
    tiles = -(-hidden // LANES)
    chunks = min(CHUNKS, tiles)
    edges = [min(-(-tiles * c // chunks) * LANES, hidden) for c in range(chunks + 1)]
    bounds = tuple(zip(edges[:-1], edges[1:]))
    widths = [hi - lo for lo, hi in bounds]
    gu_widths = [2 * w + (LANES if c == 0 else 0) for c, w in enumerate(widths)]
    out_cols = given["w_out"].shape[1]
    remote_count = (n_kv - 1) * (3 + 2 * chunks) + 2 * (n_tp - 1)
    scratch = [pltpu.VMEM(given[name].shape, given[name].dtype) for name in ORDER]
    scratch += [
        pltpu.VMEM((rows, columns), bf16),
        pltpu.VMEM((seqs, kw), f32),
        pltpu.VMEM((seqs, heads, dk, dv), bf16),
        pltpu.VMEM((seqs, kw), f32),
        pltpu.VMEM((seqs, kw), f32),
        pltpu.VMEM((seqs, kw), f32),
        pltpu.VMEM((seqs, vw), f32),
        pltpu.VMEM((n_kv, seqs, 3 * kw + LANES), bf16),
        pltpu.VMEM((n_kv - 1, seqs, 3 * kw + LANES), bf16),
        pltpu.VMEM((n_kv, seqs, 2 * vw), bf16),
        pltpu.VMEM((n_kv - 1, seqs, 2 * vw), bf16),
        pltpu.VMEM((n_kv, seqs, vw), bf16),
        pltpu.VMEM((n_tp, rows, out_cols), bf16),
        [pltpu.VMEM((n_kv, seqs, w), bf16) for w in gu_widths],
        [pltpu.VMEM((n_kv - 1, seqs, w), bf16) for w in gu_widths],
        [pltpu.VMEM((n_kv, seqs, w), bf16) for w in widths],
        pltpu.VMEM((n_tp, rows, out_cols), bf16),
        pltpu.SemaphoreType.DMA((len(ORDER) + 1,)),
        pltpu.SemaphoreType.DMA((remote_count,)),
        pltpu.SemaphoreType.DMA((remote_count,)),
    ]
    cfg = (n_kv, n_tp, ORDER, bounds)
    return pl.pallas_call(
        functools.partial(kernel, cfg),
        out_shape=jax.ShapeDtypeStruct((rows, columns), bf16),
        in_specs=[pl.BlockSpec(memory_space=pltpu.SMEM)]
        + [pl.BlockSpec(memory_space=pl.ANY)] * len(ORDER),
        out_specs=pl.BlockSpec(memory_space=pl.ANY),
        scratch_shapes=scratch,
        compiler_params=pltpu.CompilerParams(collective_id=0, has_side_effects=True),
        name="layer",
    )(lengths, *[given[name] for name in ORDER])


NAMES = (
    "tokens",
    "lengths",
    "state",
    "key_block",
    "value_block",
    "cum_decay",
    "step_decay",
    "g_mix",
    "w_query",
    "w_key",
    "w_value",
    "w_outgate",
    "w_decay",
    "g_heads",
    "w_out",
    "g_ffn",
    "w_gate",
    "w_up",
    "w_down",
)


def solution(mesh):
    def call(*arrays):
        given = dict(zip(NAMES, arrays))
        lengths = given.pop("lengths")
        return body(mesh.shape["kv"], mesh.shape["tp"], lengths, given)

    return jax.shard_map(
        call,
        mesh=mesh,
        in_specs=(
            P("grp", "kv"),
            P(("grp", "kv")),
            P(("grp", "kv"), "tp", None, None),
            P(("grp", "kv"), "tp", None, None),
            P(("grp", "kv"), "tp", None, None),
            P(("grp", "kv"), "tp", None, None),
            P(("grp", "kv"), "tp"),
            P("kv"),
            P("kv", "tp"),
            P("kv", "tp"),
            P("kv", "tp"),
            P("kv", "tp"),
            P("kv", "tp"),
            P("tp"),
            P("tp", "kv"),
            P("kv"),
            P("kv", "tp"),
            P("kv", "tp"),
            P("tp", "kv"),
        ),
        out_specs=P("grp", "kv"),
        check_vma=False,
    )
```

profile of v0, /device:TPU:0, one launch (start us, length us, event | category | flops | bytes accessed | tf_op | source)
XLA Modules:
  0.0 40.7 jit_solution(14134200039126215864)
XLA Ops:
  0.0 39.3 %layer.1 = bf16[64,512]{1,0:T(8,128)(2,1)} custom-call(s32[16]{0:T(128)} %lengths.1, bf16[64,512]{1,0:T(8,128)(2,1)} %refs_0_.1, bf16[512]{0:T(512)(128)(2,1)} %refs_1_.1, bf16[512,256]{1,0:T(8,128)(2,1)} %refs_2_.1, bf16[512,256]{1,0:T(8,128)(2,1)} %refs_3_.1, bf16[512,256]{1,0:T(8,128)(2,1)} %refs_4_.1, bf16[512,512]{1,0:T(8,128)(2,1)} %refs_5_.1, ...), custom_call_target="tpu_custom_call" | custom-call | tf_op jit(solution)/shard_map/layer/pallas_call | solution.py:358
  39.3 1.5 %copy.21 = bf16[64,512]{1,0:T(8,128)(2,1)} copy(bf16[64,512]{1,0:T(8,128)(2,1)} %layer.1) | data formatting | bytes 131072
where the time goes:
time: 40.9 us; the launch traced here: 40.7 us
  Pallas kernels  39.3 us (96%)
  local copies, waits for them, and re-layouts  1.47 us (4%)
    pallas_call x1, Pallas kernels, body(): pl.pallas_call(functools.partial(kernel, cfg), out_shape=jax.ShapeDtypeSt...  39.3 us
    unnamed x1, local copies, waits for them, and re-layouts  1.47 us

commit v1 on v0

--- a/solution.py
+++ b/solution.py
@@ -288,10 +288,7 @@
     total = down_all[0].astype(f32)
     for t in range(1, n_tp):
         total = total + down_all[t].astype(f32)
-    out_vm[...] = (middle + total).astype(bf16)
-    result = pltpu.make_async_copy(out_vm, out_hbm, local_sem.at[count])
-    result.start()
-    result.wait()
+    out_hbm[...] = (middle + total).astype(bf16)
 
 
 ORDER = (
@@ -357,10 +354,10 @@
     cfg = (n_kv, n_tp, ORDER, bounds)
     return pl.pallas_call(
         functools.partial(kernel, cfg),
-        out_shape=jax.ShapeDtypeStruct((rows, columns), bf16),
+        out_shape=pltpu.VMEM((rows, columns), bf16),
         in_specs=[pl.BlockSpec(memory_space=pltpu.SMEM)]
-        + [pl.BlockSpec(memory_space=pl.ANY)] * len(ORDER),
-        out_specs=pl.BlockSpec(memory_space=pl.ANY),
+        + [pl.BlockSpec(memory_space=pltpu.HBM)] * len(ORDER),
+        out_specs=pl.BlockSpec(memory_space=pltpu.VMEM),
         scratch_shapes=scratch,
         compiler_params=pltpu.CompilerParams(collective_id=0, has_side_effects=True),
         name="layer",

time: 40.9 us -> 39.4 us (0.963)
  local copies, waits for them, and re-layouts: 1.47 us -> 0.63 us
  Pallas kernels: 39.3 us -> 38.6 us
    unnamed x1, local copies, waits for them, and re-layouts: 1.47 us -> 0.63 us
    pallas_call x1, Pallas kernels: 39.3 us -> 38.6 us  [body(): pl.pallas_call(functools.partial(kernel, cfg), out_shape=pltpu.VMEM((rows...]
where the time goes in v1:
time: 39.4 us; the launch traced here: 39.3 us
  Pallas kernels  38.6 us (98%)
  local copies, waits for them, and re-layouts  0.63 us (2%)
    pallas_call x1, Pallas kernels, body(): pl.pallas_call(functools.partial(kernel, cfg), out_shape=pltpu.VMEM((rows...  38.6 us

profile of v1, /device:TPU:0, one launch (start us, length us, event | category | flops | bytes accessed | tf_op | source)
XLA Modules:
  0.0 39.3 jit_solution(203440166529078857)
XLA Ops:
  0.0 38.6 %layer.1 = bf16[64,512]{1,0:T(8,128)(2,1)S(1)} custom-call(s32[16]{0:T(128)} %lengths.1, bf16[64,512]{1,0:T(8,128)(2,1)} %refs_0_.1, bf16[512]{0:T(512)(128)(2,1)} %refs_1_.1, bf16[512,256]{1,0:T(8,128)(2,1)} %refs_2_.1, bf16[512,256]{1,0:T(8,128)(2,1)} %refs_3_.1, bf16[512,256]{1,0:T(8,128)(2,1)} %refs_4_.1, bf16[512,512]{1,0:T(8,128)(2,1)} %refs_5_.1, ...), custom_call_target="tpu_custom_call" | custom-call | tf_op jit(solution)/shard_map/layer/pallas_call | solution.py:355
  38.6 0.6 %copy.21 = bf16[64,512]{1,0:T(8,128)(2,1)} copy(bf16[64,512]{1,0:T(8,128)(2,1)S(1)} %layer.1) | data formatting | bytes 131072

commit v2 on v1

v2 whole, which is shorter than its diff:
```python
import functools

import jax
import jax.numpy as jnp
from jax import lax
from jax.experimental import pallas as pl
from jax.experimental.pallas import tpu as pltpu
from jax.sharding import PartitionSpec as P

f32 = jnp.float32
bf16 = jnp.bfloat16
epsilon = 1e-06
temper = 16.0
LANES = 128
MESH = pl.DeviceIdType.MESH


def silu(v):
    return v / (1.0 + jnp.exp(-v))


def far_first(n):
    return sorted(range(1, n), key=lambda o: (-min(o, n - o), -o))


def split_hi_lo(total):
    lane = lax.broadcasted_iota(jnp.int32, (total.shape[0], LANES), 1)
    wide = jnp.broadcast_to(total, (total.shape[0], LANES))
    high = wide.astype(bf16).astype(f32)
    return jnp.where(lane < LANES // 2, high, wide - high).astype(bf16)


def join_hi_lo(block):
    return block[:, :1] + block[:, LANES // 2 : LANES // 2 + 1]


def kernel(
    cfg,
    lengths,
    *refs,
):
    (n_kv, n_tp, names, bounds, parts) = cfg
    count = len(names)
    hbm = dict(zip(names, refs[:count]))
    out_ref = refs[count]
    rest = refs[count + 1 :]
    vm = dict(zip(names, rest[:count]))
    (
        td_base,
        state_bf,
        q_ref,
        td_ref,
        qe_ref,
        head_ref,
        a_send,
        a_recv,
        b_send,
        b_recv,
        a_merge,
        b_merge,
        mixed_all,
        attn_all,
        gu_send,
        gu_recv,
        gu_merge,
        hid_all,
        down_all,
        local_sem,
        send_sem,
        recv_sem,
    ) = rest[count:]

    kv = lax.axis_index("kv")
    tp = lax.axis_index("tp")
    seqs, heads, dk, dv = vm["state"].shape
    block_len = vm["key_block"].shape[2]
    width = vm["tokens"].shape[1] * n_kv
    kw = heads * dk
    vw = heads * dv
    sub = seqs // parts
    rows = n_kv * sub

    copies = {}
    for index, name in enumerate(names):
        copies[name] = pltpu.make_async_copy(hbm[name], vm[name], local_sem.at[index])
    for name in names[:EARLY]:
        copies[name].start()

    barrier = pltpu.get_barrier_semaphore()
    for o in range(1, n_kv):
        pl.semaphore_signal(
            barrier, inc=1, device_id={"kv": lax.rem(kv + o, n_kv)}, device_id_type=MESH
        )
    for o in range(1, n_tp):
        pl.semaphore_signal(
            barrier, inc=1, device_id={"tp": lax.rem(tp + o, n_tp)}, device_id_type=MESH
        )

    def gain(name):
        return vm[name][...].astype(f32).reshape(1, -1)

    sem_next = [0]
    sends = []

    def claim(number):
        first = sem_next[0]
        sem_next[0] += number
        return first

    def described(src, dst, axis, target, sent, received):
        return pltpu.make_async_remote_copy(
            src_ref=src,
            dst_ref=dst,
            send_sem=send_sem.at[sent],
            recv_sem=recv_sem.at[received],
            device_id={axis: target},
            device_id_type=MESH,
        )

    def remote(src, dst, axis, target):
        index = claim(1)
        copy = described(src, dst, axis, target, index, index)
        copy.start()
        sends.append((None, copy))
        return copy

    line = n_kv == 4 and n_tp % 2 == 0
    paired = lax.rem(tp, 2) == 1
    outer = lax.rem(kv, 3) == 0
    inner = lax.rem(kv, 3) != 0
    side = kv // 2
    partner = kv + 1 - 2 * lax.rem(kv, 2)
    far_inner = 2 - side
    far_outer = 3 - 3 * side

    def when(condition, action):
        if condition is None:
            action()
        else:
            pl.when(condition)(action)

    def launch(condition, copy):
        when(condition, copy.start)
        sends.append((condition, copy))

    paired_outer = jnp.logical_and(paired, outer)
    paired_inner = jnp.logical_and(paired, inner)
    single = jnp.logical_not(paired)

    def sum_start(send, recv, merge, merged):
        if not line or not merged:
            return (scatter(send, recv), None)
        base = claim(5)
        launch(
            paired_outer,
            described(send.at[far_outer], merge.at[0], "kv", partner, base + 1, base + 1),
        )
        launch(
            paired_outer,
            described(send.at[far_inner], merge.at[1], "kv", partner, base + 2, base + 2),
        )
        launch(paired, described(send.at[partner], recv.at[0], "kv", partner, base, base))
        for index, o in enumerate(far_first(n_kv)):
            target = lax.rem(kv + o, n_kv)
            launch(
                single,
                described(send.at[target], recv.at[o - 1], "kv", target, base + index, base + o - 1),
            )
        return (base, (send, recv, merge))

    def sum_merge(started):
        base, refs = started
        if refs is None:
            return
        send, recv, merge = refs

        def step(slot, target, sent):
            described(merge.at[slot], merge.at[slot], "kv", partner, 0, base + 1 + slot).wait_recv()
            total = send[target].astype(f32) + merge[slot].astype(f32)
            send[target] = total.astype(bf16)
            described(send.at[target], recv.at[1], "kv", target, sent, base + 3).start()

        def both():
            step(0, far_outer, base + 3)
            step(1, far_inner, base + 4)

        when(paired_inner, both)
        for target, sent in ((far_outer, base + 3), (far_inner, base + 4)):
            copy = described(send.at[target], recv.at[1], "kv", target, sent, base + 3)
            sends.append((paired_inner, copy))

    def sum_wait(started):
        base, refs = started
        if refs is None:
            wait_all(base)
            return
        send, recv, merge = refs

        def pair():
            for slot, received in ((0, base), (1, base + 3)):
                described(recv.at[slot], recv.at[slot], "kv", partner, 0, received).wait_recv()

        def each():
            for slot in range(n_kv - 1):
                described(recv.at[slot], recv.at[slot], "kv", partner, 0, base + slot).wait_recv()

        when(paired, pair)
        when(single, each)

    def spread_start(buffer, relayed):
        if not line or not relayed:
            return (gather(buffer, "kv"), None)
        base = claim(5)

        def sent_to(condition, target, sent, received):
            copy = described(buffer.at[kv], buffer.at[kv], "kv", target, sent, received)
            launch(condition, copy)

        sent_to(paired_outer, far_inner, base + 1, base + 1)
        sent_to(paired_inner, far_inner, base + 1, base + 2)
        sent_to(paired, partner, base, base)
        for index, o in enumerate(far_first(n_kv)):
            sent_to(single, lax.rem(kv + o, n_kv), base + index, base + o - 1)
        return (base, buffer)

    def landed(buffer, owner, received):
        described(buffer.at[owner], buffer.at[owner], "kv", partner, 0, received).wait_recv()

    def spread_pass(started):
        base, buffer = started
        if buffer is None:
            return

        def passed(owner, sent, received):
            return described(buffer.at[owner], buffer.at[owner], "kv", partner, sent, received)

        hops = (passed(far_inner, base + 4, base + 2), passed(far_outer, base + 3, base + 1))

        def both():
            landed(buffer, far_inner, base + 2)
            hops[0].start()
            landed(buffer, far_outer, base + 1)
            hops[1].start()

        when(paired_inner, both)
        sends.extend((paired_inner, copy) for copy in hops)

    def spread_wait(started):
        base, buffer = started
        if buffer is None:
            wait_all(base)
            return

        def far():
            landed(buffer, far_inner, base + 2)
            landed(buffer, far_outer, base + 1)

        def each():
            for o in range(1, n_kv):
                landed(buffer, lax.rem(kv + n_kv - o, n_kv), base + o - 1)

        when(paired, lambda: landed(buffer, partner, base))
        when(paired_outer, far)
        when(single, each)

    def scatter(send, recv):
        result = []
        for o in far_first(n_kv):
            target = lax.rem(kv + o, n_kv)
            result.append(remote(send.at[target], recv.at[o - 1], "kv", target))
        return result

    def gather_tp(buffer):
        if n_tp % 2:
            return gather(buffer, "tp")
        base = claim(n_tp - 1)
        orders = []
        for me in range(2):
            orders.append(sorted(range(1, n_tp), key=lambda o: (me + o in (0, 1, n_tp), (me + o) % 2, o)))
        for even, odd in zip(*orders):
            o = even + (odd - even) * lax.rem(tp, 2)
            target = lax.rem(tp + o, n_tp)
            sem = base + o - 1
            launch(None, described(buffer.at[tp], buffer.at[tp], "tp", target, sem, sem))
        return [
            described(buffer.at[tp], buffer.at[lax.rem(tp + n_tp - o, n_tp)], "tp", tp, 0, base + o - 1)
            for o in range(1, n_tp)
        ]

    def gather(buffer, axis):
        me, n = (kv, n_kv) if axis == "kv" else (tp, n_tp)
        return [
            remote(buffer.at[me], buffer.at[me], axis, lax.rem(me + o, n)) for o in far_first(n)
        ]

    def wait_all(started):
        for copy in started:
            copy.wait_recv()

    def store_all(buffer, lo, value):
        for p in range(parts):
            for d in range(n_kv):
                first = d * seqs + p * sub
                buffer[p, d, :, lo : lo + value.shape[1]] = value[first : first + sub]

    def store_rows(buffer, p, lo, value):
        for d in range(n_kv):
            buffer[p, d, :, lo : lo + value.shape[1]] = value[d * sub : (d + 1) * sub]

    def rows_of(value, p):
        pieces = [value[d * seqs + p * sub : d * seqs + (p + 1) * sub] for d in range(n_kv)]
        return jnp.concatenate(pieces, axis=0)

    def joined(block):
        return block.astype(f32).reshape(rows, block.shape[2]).astype(bf16)

    def reduced(send, recv, p, lo, hi):
        total = send[p, kv, :, lo:hi].astype(f32)
        for o in range(n_kv - 1):
            total = total + recv[p, o, :, lo:hi].astype(f32)
        return total

    if line:

        @pl.when(paired)
        def _():
            for buffer, chosen in ((a_recv, MERGE_A), (b_recv, MERGE_B)):
                for p in chosen:
                    buffer[p, n_kv - 2] = jnp.zeros(buffer.shape[2:], bf16)
            for buffer in gu_recv:
                for p in MERGE_GU:
                    buffer[p, n_kv - 2] = jnp.zeros(buffer.shape[2:], bf16)

    copies["tokens"].wait()
    copies["g_mix"].wait()
    inputs = vm["tokens"][...].astype(f32)
    scaled = (inputs * gain("g_mix")).astype(bf16)
    store_all(a_send, 3 * kw, split_hi_lo(jnp.sum(inputs * inputs, axis=1, keepdims=True)))
    for index, name in enumerate(("w_query", "w_key", "w_decay")):
        copies[name].wait()
        part = jnp.dot(scaled, vm[name][...], preferred_element_type=f32)
        store_all(a_send, index * kw, part.astype(bf16))
    for name in names[EARLY:]:
        copies[name].start()
    pl.semaphore_wait(barrier, n_kv - 1 + n_tp - 1)
    if line and HOLD:

        @pl.when(paired)
        def _():
            pl.delay(HOLD)

    def start_a(p):
        return sum_start(a_send.at[p], a_recv.at[p], a_merge.at[p], p in MERGE_A)

    def start_b(p):
        return sum_start(b_send.at[p], b_recv.at[p], b_merge.at[p], p in MERGE_B)

    sent_a = [start_a(0)]
    for index, name in enumerate(("w_value", "w_outgate")):
        copies[name].wait()
        part = jnp.dot(scaled, vm[name][...], preferred_element_type=f32)
        store_all(b_send, index * vw, part.astype(bf16))
    sent_b = [start_b(0)]
    for p in range(1, parts):
        sent_a.append(start_a(p))
        sent_b.append(start_b(p))

    copies["cum_decay"].wait()
    copies["state"].wait()
    ordinal = lax.broadcasted_iota(jnp.int32, (block_len, dk), 0)

    group = 8 if sub % 8 == 0 else sub

    def prepare(step, carry):
        base = pl.multiple_of(step * group, group)
        for h in range(heads):
            ends = []
            for inner in range(group):
                s = base + inner
                live = lax.rem(lengths[s], block_len)
                picked = jnp.where(ordinal == live - 1, vm["cum_decay"][s, h], 0.0)
                ends.append(jnp.sum(picked, axis=0, keepdims=True))
                state_bf[s, h] = vm["state"][s, h].astype(bf16)
            td_base[pl.ds(base, group), h * dk : (h + 1) * dk] = jnp.concatenate(ends, axis=0)
        return carry

    lax.fori_loop(0, seqs // group, prepare, 0)
    for name in ("step_decay", "key_block", "value_block", "g_heads"):
        copies[name].wait()

    live_ordinal = lax.broadcasted_iota(jnp.int32, (block_len, 1), 0)

    def attend(step, carry):
        base = pl.multiple_of(step * group, group)
        for h in range(heads):
            cols = slice(h * dk, (h + 1) * dk)
            qs = q_ref[pl.ds(base, group), cols]
            tds = td_ref[pl.ds(base, group), cols]
            qes = qe_ref[pl.ds(base, group), cols]
            outs = []
            for inner in range(group):
                s = base + inner
                live = lax.rem(lengths[s], block_len)
                left = jnp.broadcast_to(qes[inner : inner + 1], (16, dk)).astype(bf16)
                carried = jnp.dot(left, state_bf[s, h], preferred_element_type=f32)[:1]
                scores = jnp.sum(
                    qs[inner : inner + 1]
                    * vm["key_block"][s, h].astype(f32)
                    * jnp.exp(tds[inner : inner + 1] - vm["cum_decay"][s, h]),
                    axis=1,
                    keepdims=True,
                )
                scores = jnp.where(live_ordinal < live, scores, 0.0)
                in_block = jnp.sum(
                    scores * vm["value_block"][s, h].astype(f32), axis=0, keepdims=True
                )
                outs.append(carried + in_block)
            head_ref[pl.ds(base, group), h * dv : (h + 1) * dv] = jnp.concatenate(outs, axis=0)
        return carry

    for p in range(parts):
        sum_merge(sent_a[p])
        sum_merge(sent_b[p])
    sent_mixed = []
    for p in range(parts):
        own_rows = slice(p * sub, (p + 1) * sub)
        sum_wait(sent_a[p])
        square = join_hi_lo(reduced(a_send, a_recv, p, 3 * kw, 3 * kw + LANES))
        inverse = lax.rsqrt(square / width + epsilon)
        query = reduced(a_send, a_recv, p, 0, kw) * inverse * dk ** (-0.5)
        keys_new = reduced(a_send, a_recv, p, kw, 2 * kw) * inverse
        decay_pre = reduced(a_send, a_recv, p, 2 * kw, 3 * kw) * inverse
        log_sigmoid = jnp.minimum(decay_pre, 0.0) - jnp.log(1.0 + jnp.exp(-jnp.abs(decay_pre)))
        log_step = log_sigmoid / temper + vm["step_decay"][own_rows]
        token_decay = td_base[own_rows] + log_step
        q_ref[own_rows] = query
        td_ref[own_rows] = token_decay
        qe_ref[own_rows] = query * jnp.exp(token_decay)
        lax.fori_loop(p * sub // group, (p + 1) * sub // group, attend, 0)
        sum_wait(sent_b[p])
        for h in range(heads):
            cols = slice(h * dv, (h + 1) * dv)
            keys = slice(h * dk, (h + 1) * dk)
            values_new = reduced(b_send, b_recv, p, h * dv, (h + 1) * dv) * inverse
            out_gate = reduced(b_send, b_recv, p, vw + h * dv, vw + (h + 1) * dv) * inverse
            own = jnp.sum(query[:, keys] * keys_new[:, keys], axis=1, keepdims=True)
            head_out = head_ref[own_rows, cols] + own * values_new
            scale = lax.rsqrt(jnp.mean(head_out * head_out, axis=1, keepdims=True) + epsilon)
            normed = head_out * scale * gain("g_heads")[:, cols]
            mixed_all[p, kv, :, cols] = (normed * silu(out_gate)).astype(bf16)
        sent_mixed.append(gather(mixed_all.at[p], "kv"))

    copies["w_out"].wait()
    sent_attn = []
    for p in range(parts):
        wait_all(sent_mixed[p])
        part = jnp.dot(joined(mixed_all[p]), vm["w_out"][...], preferred_element_type=f32)
        attn_all[p, tp] = part.astype(bf16)
        sent_attn.append(gather_tp(attn_all.at[p]))

    copies["g_ffn"].wait()
    copies["w_gate"].wait()
    copies["w_up"].wait()
    middles = []
    sent_gu = []
    for p in range(parts):
        wait_all(sent_attn[p])
        attention = attn_all[p, 0].astype(f32)
        for t in range(1, n_tp):
            attention = attention + attn_all[p, t].astype(f32)
        middle = (rows_of(inputs, p) + attention).astype(bf16).astype(f32)
        normed_mid = (middle * gain("g_ffn")).astype(bf16)
        middles.append(middle)
        sent_gu.append([])
        for c, (lo, hi) in enumerate(bounds):
            if c == 0:
                square = jnp.sum(middle * middle, axis=1, keepdims=True)
                store_rows(gu_send[c], p, 2 * (hi - lo), split_hi_lo(square))
            for index, name in enumerate(("w_gate", "w_up")):
                part = jnp.dot(normed_mid, vm[name][:, lo:hi], preferred_element_type=f32)
                store_rows(gu_send[c], p, index * (hi - lo), part.astype(bf16))
            refs = (gu_send[c].at[p], gu_recv[c].at[p], gu_merge[c].at[p])
            sent_gu[p].append(sum_start(*refs, p in MERGE_GU))
    order = [(p, c) for p in range(parts) for c in range(len(bounds))]
    ahead = order[len(bounds) :]
    for c in range(len(bounds)):
        sum_merge(sent_gu[0][c])
    sent_hid = [[] for _ in range(parts)]
    passing = []
    for p, c in order:
        lo, hi = bounds[c]
        w = hi - lo
        sum_wait(sent_gu[p][c])
        if c == 0:
            total = join_hi_lo(reduced(gu_send[c], gu_recv[c], p, 2 * w, 2 * w + LANES))
            mid_inverse = lax.rsqrt(total / width + epsilon)
        gate = reduced(gu_send[c], gu_recv[c], p, 0, w) * mid_inverse
        up = reduced(gu_send[c], gu_recv[c], p, w, 2 * w) * mid_inverse
        hid_all[c][p, kv] = (silu(gate) * up).astype(bf16)
        sent_hid[p].append(spread_start(hid_all[c].at[p], p in RELAY))
        passing.append(sent_hid[p][c])
        if ahead:
            q, e = ahead.pop(0)
            sum_merge(sent_gu[q][e])
        elif len(passing) > 1:
            spread_pass(passing.pop(0))
    copies["w_down"].wait()
    sent_down = []
    for p in range(parts):
        if p == parts - 1:
            for started in passing:
                spread_pass(started)
        down = None
        for c, (lo, hi) in enumerate(bounds):
            spread_wait(sent_hid[p][c])
            part = jnp.dot(joined(hid_all[c][p]), vm["w_down"][lo:hi], preferred_element_type=f32)
            down = part if down is None else down + part
        down_all[p, tp] = down.astype(bf16)
        sent_down.append(gather_tp(down_all.at[p]))
    finals = []
    for p in range(parts):
        wait_all(sent_down[p])
        total = down_all[p, 0].astype(f32)
        for t in range(1, n_tp):
            total = total + down_all[p, t].astype(f32)
        finals.append(middles[p] + total)
    ordered = [finals[p][d * sub : (d + 1) * sub] for d in range(n_kv) for p in range(parts)]
    out_ref[...] = jnp.concatenate(ordered, axis=0).astype(bf16)
    for condition, copy in sends:
        when(condition, copy.wait_send)


ORDER = (
    "tokens",
    "g_mix",
    "w_query",
    "w_key",
    "w_decay",
    "w_value",
    "w_outgate",
    "cum_decay",
    "state",
    "step_decay",
    "key_block",
    "value_block",
    "g_heads",
    "w_out",
    "g_ffn",
    "w_gate",
    "w_up",
    "w_down",
)
CHUNKS = 2
PARTS = 2
HOLD = 0
RELAY = (0,)
MERGE_A = (0, 1)
MERGE_B = (0, 1)
MERGE_GU = (0, 1)
EARLY = 7


def body(n_kv, n_tp, lengths, given):
    rows, columns = given["tokens"].shape
    seqs, heads, dk, dv = given["state"].shape
    kw, vw = heads * dk, heads * dv
    hidden = given["w_gate"].shape[1]
    tiles = -(-hidden // LANES)
    chunks = min(CHUNKS, tiles)
    edges = [min(-(-tiles * c // chunks) * LANES, hidden) for c in range(chunks + 1)]
    bounds = tuple(zip(edges[:-1], edges[1:]))
    widths = [hi - lo for lo, hi in bounds]
    gu_widths = [2 * w + (LANES if c == 0 else 0) for c, w in enumerate(widths)]
    out_cols = given["w_out"].shape[1]
    parts = PARTS if seqs % (8 * PARTS) == 0 else 1
    sub = seqs // parts
    each = max(n_kv - 1, 5)
    remote_count = parts * (each * (3 + 2 * chunks) + 2 * (n_tp - 1))
    scratch = [pltpu.VMEM(given[name].shape, given[name].dtype) for name in ORDER]
    scratch += [
        pltpu.VMEM((seqs, kw), f32),
        pltpu.VMEM((seqs, heads, dk, dv), bf16),
        pltpu.VMEM((seqs, kw), f32),
        pltpu.VMEM((seqs, kw), f32),
        pltpu.VMEM((seqs, kw), f32),
        pltpu.VMEM((seqs, vw), f32),
        pltpu.VMEM((parts, n_kv, sub, 3 * kw + LANES), bf16),
        pltpu.VMEM((parts, n_kv - 1, sub, 3 * kw + LANES), bf16),
        pltpu.VMEM((parts, n_kv, sub, 2 * vw), bf16),
        pltpu.VMEM((parts, n_kv - 1, sub, 2 * vw), bf16),
        pltpu.VMEM((parts, 2, sub, 3 * kw + LANES), bf16),
        pltpu.VMEM((parts, 2, sub, 2 * vw), bf16),
        pltpu.VMEM((parts, n_kv, sub, vw), bf16),
        pltpu.VMEM((parts, n_tp, n_kv * sub, out_cols), bf16),
        [pltpu.VMEM((parts, n_kv, sub, w), bf16) for w in gu_widths],
        [pltpu.VMEM((parts, n_kv - 1, sub, w), bf16) for w in gu_widths],
        [pltpu.VMEM((parts, 2, sub, w), bf16) for w in gu_widths],
        [pltpu.VMEM((parts, n_kv, sub, w), bf16) for w in widths],
        pltpu.VMEM((parts, n_tp, n_kv * sub, out_cols), bf16),
        pltpu.SemaphoreType.DMA((len(ORDER),)),
        pltpu.SemaphoreType.DMA((remote_count,)),
        pltpu.SemaphoreType.DMA((remote_count,)),
    ]
    cfg = (n_kv, n_tp, ORDER, bounds, parts)
    return pl.pallas_call(
        functools.partial(kernel, cfg),
        out_shape=pltpu.VMEM((rows, columns), bf16),
        in_specs=[pl.BlockSpec(memory_space=pltpu.SMEM)]
        + [pl.BlockSpec(memory_space=pltpu.HBM)] * len(ORDER),
        out_specs=pl.BlockSpec(memory_space=pltpu.VMEM),
        scratch_shapes=scratch,
        compiler_params=pltpu.CompilerParams(collective_id=0, has_side_effects=True),
        name="layer",
    )(lengths, *[given[name] for name in ORDER])


NAMES = (
    "tokens",
    "lengths",
    "state",
    "key_block",
    "value_block",
    "cum_decay",
    "step_decay",
    "g_mix",
    "w_query",
    "w_key",
    "w_value",
    "w_outgate",
    "w_decay",
    "g_heads",
    "w_out",
    "g_ffn",
    "w_gate",
    "w_up",
    "w_down",
)


def solution(mesh):
    def call(*arrays):
        given = dict(zip(NAMES, arrays))
        lengths = given.pop("lengths")
        return body(mesh.shape["kv"], mesh.shape["tp"], lengths, given)

    return jax.shard_map(
        call,
        mesh=mesh,
        in_specs=(
            P("grp", "kv"),
            P(("grp", "kv")),
            P(("grp", "kv"), "tp", None, None),
            P(("grp", "kv"), "tp", None, None),
            P(("grp", "kv"), "tp", None, None),
            P(("grp", "kv"), "tp", None, None),
            P(("grp", "kv"), "tp"),
            P("kv"),
            P("kv", "tp"),
            P("kv", "tp"),
            P("kv", "tp"),
            P("kv", "tp"),
            P("kv", "tp"),
            P("tp"),
            P("tp", "kv"),
            P("kv"),
            P("kv", "tp"),
            P("kv", "tp"),
            P("tp", "kv"),
        ),
        out_specs=P("grp", "kv"),
        check_vma=False,
    )
```

time: 39.4 us -> 37.7 us (0.957)
  Pallas kernels: 38.6 us -> 36.9 us
    pallas_call x1, Pallas kernels: 38.6 us -> 36.9 us  [body(): pl.pallas_call(functools.partial(kernel, cfg), out_shape=pltpu.VMEM((rows...]
where the time goes in v2:
time: 37.7 us; the launch traced here: 37.6 us
  Pallas kernels  36.9 us (98%)
  local copies, waits for them, and re-layouts  0.63 us (2%)
    pallas_call x1, Pallas kernels, body(): pl.pallas_call(functools.partial(kernel, cfg), out_shape=pltpu.VMEM((rows...  36.9 us

profile of v2, /device:TPU:0, one launch (start us, length us, event | category | flops | bytes accessed | tf_op | source)
XLA Modules:
  0.0 37.6 jit_solution(17058678242811891866)
XLA Ops:
  0.0 36.9 %layer.1 = bf16[64,512]{1,0:T(8,128)(2,1)S(1)} custom-call(s32[16]{0:T(128)} %lengths.1, bf16[64,512]{1,0:T(8,128)(2,1)} %refs_0_.1, bf16[512]{0:T(512)(128)(2,1)} %refs_1_.1, bf16[512,256]{1,0:T(8,128)(2,1)} %refs_2_.1, bf16[512,256]{1,0:T(8,128)(2,1)} %refs_3_.1, bf16[512,256]{1,0:T(8,128)(2,1)} %refs_4_.1, bf16[512,512]{1,0:T(8,128)(2,1)} %refs_5_.1, ...), custom_call_target="tpu_custom_call" | custom-call | tf_op jit(solution)/shard_map/layer/pallas_call | solution.py:605
  36.9 0.6 %copy.21 = bf16[64,512]{1,0:T(8,128)(2,1)} copy(bf16[64,512]{1,0:T(8,128)(2,1)S(1)} %layer.1) | data formatting | bytes 131072

commit v3 on v2

--- a/solution.py
+++ b/solution.py
@@ -36,14 +36,13 @@
 
 def kernel(
     cfg,
-    lengths,
     *refs,
 ):
     (n_kv, n_tp, names, bounds, parts) = cfg
     count = len(names)
     hbm = dict(zip(names, refs[:count]))
-    out_ref = refs[count]
-    rest = refs[count + 1 :]
+    (lengths_hbm, out_ref, lengths) = refs[count : count + 3]
+    rest = refs[count + 3 :]
     vm = dict(zip(names, rest[:count]))
     (
         td_base,
@@ -80,12 +79,6 @@
     sub = seqs // parts
     rows = n_kv * sub
 
-    copies = {}
-    for index, name in enumerate(names):
-        copies[name] = pltpu.make_async_copy(hbm[name], vm[name], local_sem.at[index])
-    for name in names[:EARLY]:
-        copies[name].start()
-
     barrier = pltpu.get_barrier_semaphore()
     for o in range(1, n_kv):
         pl.semaphore_signal(
@@ -96,16 +89,30 @@
             barrier, inc=1, device_id={"tp": lax.rem(tp + o, n_tp)}, device_id_type=MESH
         )
 
+    copies = {}
+    for index, name in enumerate(names):
+        reused = EARLY <= index < EARLY + FIRST
+        sem = index if index < EARLY else index - (EARLY if reused else FIRST)
+        copies[name] = pltpu.make_async_copy(hbm[name], vm[name], local_sem.at[sem])
+    for name in names[:EARLY]:
+        copies[name].start()
+    copies["lengths"] = pltpu.make_async_copy(lengths_hbm, lengths, local_sem.at[count - FIRST])
+
     def gain(name):
         return vm[name][...].astype(f32).reshape(1, -1)
 
-    sem_next = [0]
-    sends = []
-
-    def claim(number):
-        first = sem_next[0]
-        sem_next[0] += number
-        return first
+    steps = max(2, len(bounds))
+    per_recv = 3 * steps + 2 * len(bounds) + 3
+    per_send = steps + len(bounds) + 1
+
+    def sum_sems(p, k):
+        return (p * per_send + k, p * per_recv + 3 * k)
+
+    def spread_sems(p, c):
+        return (p * per_send + steps + c, p * per_recv + 3 * steps + 2 * c)
+
+    def tp_sems(p):
+        return (p * per_send + steps + len(bounds), (p + 1) * per_recv - 3)
 
     def described(src, dst, axis, target, sent, received):
         return pltpu.make_async_remote_copy(
@@ -117,21 +124,18 @@
             device_id_type=MESH,
         )
 
-    def remote(src, dst, axis, target):
-        index = claim(1)
-        copy = described(src, dst, axis, target, index, index)
-        copy.start()
-        sends.append((None, copy))
-        return copy
-
     line = n_kv == 4 and n_tp % 2 == 0
     paired = lax.rem(tp, 2) == 1
+    single = lax.rem(tp, 2) == 0
     outer = lax.rem(kv, 3) == 0
     inner = lax.rem(kv, 3) != 0
     side = kv // 2
     partner = kv + 1 - 2 * lax.rem(kv, 2)
     far_inner = 2 - side
     far_outer = 3 - 3 * side
+    paired_outer = jnp.logical_and(paired, outer)
+    paired_inner = jnp.logical_and(paired, inner)
+    drains = []
 
     def when(condition, action):
         if condition is None:
@@ -139,163 +143,125 @@
         else:
             pl.when(condition)(action)
 
-    def launch(condition, copy):
-        when(condition, copy.start)
-        sends.append((condition, copy))
-
-    paired_outer = jnp.logical_and(paired, outer)
-    paired_inner = jnp.logical_and(paired, inner)
-    single = jnp.logical_not(paired)
-
-    def sum_start(send, recv, merge, merged):
-        if not line or not merged:
-            return (scatter(send, recv), None)
-        base = claim(5)
-        launch(
-            paired_outer,
-            described(send.at[far_outer], merge.at[0], "kv", partner, base + 1, base + 1),
-        )
-        launch(
-            paired_outer,
-            described(send.at[far_inner], merge.at[1], "kv", partner, base + 2, base + 2),
-        )
-        launch(paired, described(send.at[partner], recv.at[0], "kv", partner, base, base))
-        for index, o in enumerate(far_first(n_kv)):
-            target = lax.rem(kv + o, n_kv)
-            launch(
-                single,
-                described(send.at[target], recv.at[o - 1], "kv", target, base + index, base + o - 1),
-            )
-        return (base, (send, recv, merge))
+    def arrived(ref, received):
+        described(ref, ref, "kv", partner if line else kv, 0, received).wait_recv()
+
+    def drain_later(condition, ref, sent):
+        drains.append((condition, described(ref, ref, "kv", partner if line else kv, sent, 0)))
+
+    def drain():
+        for condition, copy in drains:
+            when(condition, copy.wait_send)
+        drains.clear()
+
+    def sum_start(send, recv, merge, merged, p, k):
+        sent, received = sum_sems(p, k)
+        merged = merged and line
+
+        def direct():
+            for o in far_first(n_kv):
+                target = lax.rem(kv + o, n_kv)
+                described(send.at[target], recv.at[o - 1], "kv", target, sent, received).start()
+
+        def to_pair(block, ref, sem):
+            described(send.at[block], ref, "kv", partner, sent, sem).start()
+
+        def halves():
+            to_pair(far_outer, merge.at[0], received + 1)
+            to_pair(far_inner, merge.at[1], received + 2)
+
+        if merged:
+            when(paired_outer, halves)
+            when(paired, lambda: to_pair(partner, recv.at[0], received))
+            when(single, direct)
+        else:
+            direct()
+        drain_later(None, recv, sent)
+        return (send, recv, merge, merged, sent, received)
 
     def sum_merge(started):
-        base, refs = started
-        if refs is None:
-            return
-        send, recv, merge = refs
-
-        def step(slot, target, sent):
-            described(merge.at[slot], merge.at[slot], "kv", partner, 0, base + 1 + slot).wait_recv()
-            total = send[target].astype(f32) + merge[slot].astype(f32)
-            send[target] = total.astype(bf16)
-            described(send.at[target], recv.at[1], "kv", target, sent, base + 3).start()
+        send, recv, merge, merged, sent, received = started
 
         def both():
-            step(0, far_outer, base + 3)
-            step(1, far_inner, base + 4)
-
-        when(paired_inner, both)
-        for target, sent in ((far_outer, base + 3), (far_inner, base + 4)):
-            copy = described(send.at[target], recv.at[1], "kv", target, sent, base + 3)
-            sends.append((paired_inner, copy))
+            for slot, target in ((0, far_outer), (1, far_inner)):
+                arrived(merge.at[slot], received + 1 + slot)
+                total = send[target].astype(f32) + merge[slot].astype(f32)
+                send[target] = total.astype(bf16)
+                described(send.at[target], recv.at[1], "kv", target, sent, received).start()
+
+        if merged:
+            when(paired_inner, both)
 
     def sum_wait(started):
-        base, refs = started
-        if refs is None:
-            wait_all(base)
-            return
-        send, recv, merge = refs
-
-        def pair():
-            for slot, received in ((0, base), (1, base + 3)):
-                described(recv.at[slot], recv.at[slot], "kv", partner, 0, received).wait_recv()
-
-        def each():
-            for slot in range(n_kv - 1):
-                described(recv.at[slot], recv.at[slot], "kv", partner, 0, base + slot).wait_recv()
-
-        when(paired, pair)
-        when(single, each)
-
-    def spread_start(buffer, relayed):
-        if not line or not relayed:
-            return (gather(buffer, "kv"), None)
-        base = claim(5)
-
-        def sent_to(condition, target, sent, received):
-            copy = described(buffer.at[kv], buffer.at[kv], "kv", target, sent, received)
-            launch(condition, copy)
-
-        sent_to(paired_outer, far_inner, base + 1, base + 1)
-        sent_to(paired_inner, far_inner, base + 1, base + 2)
-        sent_to(paired, partner, base, base)
-        for index, o in enumerate(far_first(n_kv)):
-            sent_to(single, lax.rem(kv + o, n_kv), base + index, base + o - 1)
-        return (base, buffer)
-
-    def landed(buffer, owner, received):
-        described(buffer.at[owner], buffer.at[owner], "kv", partner, 0, received).wait_recv()
+        send, recv, merge, merged, sent, received = started
+        if merged:
+            when(paired, lambda: arrived(recv.at[0:2], received))
+            when(single, lambda: arrived(recv, received))
+        else:
+            arrived(recv, received)
+
+    def spread_start(buffer, relayed, p, c):
+        sent, received = spread_sems(p, c)
+        relayed = relayed and line
+
+        def own(target, sem):
+            described(buffer.at[kv], buffer.at[kv], "kv", target, sent, sem).start()
+
+        def direct():
+            for o in far_first(n_kv):
+                own(lax.rem(kv + o, n_kv), received)
+
+        def short():
+            own(far_inner, received + 1)
+            own(partner, received)
+
+        if relayed:
+            when(paired, short)
+            when(single, direct)
+            drain_later(paired_outer, buffer.at[0:2], sent)
+            drain_later(paired_inner, buffer, sent)
+            drain_later(single, buffer.at[0 : n_kv - 1], sent)
+        else:
+            direct()
+            drain_later(None, buffer.at[0 : n_kv - 1], sent)
+        return (buffer, relayed, sent, received)
 
     def spread_pass(started):
-        base, buffer = started
-        if buffer is None:
-            return
-
-        def passed(owner, sent, received):
-            return described(buffer.at[owner], buffer.at[owner], "kv", partner, sent, received)
-
-        hops = (passed(far_inner, base + 4, base + 2), passed(far_outer, base + 3, base + 1))
+        buffer, relayed, sent, received = started
 
         def both():
-            landed(buffer, far_inner, base + 2)
-            hops[0].start()
-            landed(buffer, far_outer, base + 1)
-            hops[1].start()
-
-        when(paired_inner, both)
-        sends.extend((paired_inner, copy) for copy in hops)
+            arrived(buffer.at[0:2], received + 1)
+            for owner in (far_inner, far_outer):
+                block = buffer.at[owner]
+                described(block, block, "kv", partner, sent, received + 1).start()
+
+        if relayed:
+            when(paired_inner, both)
 
     def spread_wait(started):
-        base, buffer = started
-        if buffer is None:
-            wait_all(base)
-            return
-
-        def far():
-            landed(buffer, far_inner, base + 2)
-            landed(buffer, far_outer, base + 1)
-
-        def each():
-            for o in range(1, n_kv):
-                landed(buffer, lax.rem(kv + n_kv - o, n_kv), base + o - 1)
-
-        when(paired, lambda: landed(buffer, partner, base))
-        when(paired_outer, far)
-        when(single, each)
-
-    def scatter(send, recv):
-        result = []
-        for o in far_first(n_kv):
-            target = lax.rem(kv + o, n_kv)
-            result.append(remote(send.at[target], recv.at[o - 1], "kv", target))
-        return result
-
-    def gather_tp(buffer):
-        if n_tp % 2:
-            return gather(buffer, "tp")
-        base = claim(n_tp - 1)
+        buffer, relayed, sent, received = started
+        if relayed:
+            when(paired, lambda: arrived(buffer.at[0], received))
+            when(paired_outer, lambda: arrived(buffer.at[0:2], received + 1))
+            when(single, lambda: arrived(buffer.at[0 : n_kv - 1], received))
+        else:
+            arrived(buffer.at[0 : n_kv - 1], received)
+
+    def gather_tp(buffer, p):
+        sent, received = tp_sems(p)
         orders = []
         for me in range(2):
-            orders.append(sorted(range(1, n_tp), key=lambda o: (me + o in (0, 1, n_tp), (me + o) % 2, o)))
+            keys = {o: (me + o in (1, n_tp), (me + o) % 2, o) for o in range(1, n_tp)}
+            orders.append(sorted(keys, key=keys.get))
         for even, odd in zip(*orders):
-            o = even + (odd - even) * lax.rem(tp, 2)
+            o = even + (odd - even) * lax.rem(tp, 2) if n_tp % 2 == 0 else even
             target = lax.rem(tp + o, n_tp)
-            sem = base + o - 1
-            launch(None, described(buffer.at[tp], buffer.at[tp], "tp", target, sem, sem))
-        return [
-            described(buffer.at[tp], buffer.at[lax.rem(tp + n_tp - o, n_tp)], "tp", tp, 0, base + o - 1)
-            for o in range(1, n_tp)
-        ]
-
-    def gather(buffer, axis):
-        me, n = (kv, n_kv) if axis == "kv" else (tp, n_tp)
-        return [
-            remote(buffer.at[me], buffer.at[me], axis, lax.rem(me + o, n)) for o in far_first(n)
-        ]
-
-    def wait_all(started):
-        for copy in started:
-            copy.wait_recv()
+            block = buffer.at[tp]
+            described(block, block, "tp", target, sent, received + 2).start()
+        drain_later(None, buffer.at[0 : n_tp - 1], sent)
+
+    def gather_wait(buffer, p):
+        arrived(buffer.at[0 : n_tp - 1], tp_sems(p)[1] + 2)
 
     def store_all(buffer, lo, value):
         for p in range(parts):
@@ -342,6 +308,7 @@
         store_all(a_send, index * kw, part.astype(bf16))
     for name in names[EARLY:]:
         copies[name].start()
+    copies["lengths"].start()
     pl.semaphore_wait(barrier, n_kv - 1 + n_tp - 1)
     if line and HOLD:
 
@@ -350,10 +317,10 @@
             pl.delay(HOLD)
 
     def start_a(p):
-        return sum_start(a_send.at[p], a_recv.at[p], a_merge.at[p], p in MERGE_A)
+        return sum_start(a_send.at[p], a_recv.at[p], a_merge.at[p], p in MERGE_A, p, 0)
 
     def start_b(p):
-        return sum_start(b_send.at[p], b_recv.at[p], b_merge.at[p], p in MERGE_B)
+        return sum_start(b_send.at[p], b_recv.at[p], b_merge.at[p], p in MERGE_B, p, 1)
 
     sent_a = [start_a(0)]
     for index, name in enumerate(("w_value", "w_outgate")):
@@ -361,12 +328,17 @@
         part = jnp.dot(scaled, vm[name][...], preferred_element_type=f32)
         store_all(b_send, index * vw, part.astype(bf16))
     sent_b = [start_b(0)]
-    for p in range(1, parts):
-        sent_a.append(start_a(p))
-        sent_b.append(start_b(p))
+    def start_later():
+        for p in range(1, parts):
+            sent_a.append(start_a(p))
+            sent_b.append(start_b(p))
+
+    if LATER == 0:
+        start_later()
 
     copies["cum_decay"].wait()
     copies["state"].wait()
+    copies["lengths"].wait()
     ordinal = lax.broadcasted_iota(jnp.int32, (block_len, dk), 0)
 
     group = 8 if sub % 8 == 0 else sub
@@ -385,6 +357,8 @@
         return carry
 
     lax.fori_loop(0, seqs // group, prepare, 0)
+    if LATER == 1:
+        start_later()
     for name in ("step_decay", "key_block", "value_block", "g_heads"):
         copies[name].wait()
 
@@ -418,13 +392,15 @@
             head_ref[pl.ds(base, group), h * dv : (h + 1) * dv] = jnp.concatenate(outs, axis=0)
         return carry
 
-    for p in range(parts):
-        sum_merge(sent_a[p])
-        sum_merge(sent_b[p])
+    sum_merge(sent_a[0])
+    sum_merge(sent_b[0])
     sent_mixed = []
     for p in range(parts):
         own_rows = slice(p * sub, (p + 1) * sub)
         sum_wait(sent_a[p])
+        if p == 0:
+            if LATER == 2:
+                start_later()
         square = join_hi_lo(reduced(a_send, a_recv, p, 3 * kw, 3 * kw + LANES))
         inverse = lax.rsqrt(square / width + epsilon)
         query = reduced(a_send, a_recv, p, 0, kw) * inverse * dk ** (-0.5)
@@ -448,15 +424,52 @@
             scale = lax.rsqrt(jnp.mean(head_out * head_out, axis=1, keepdims=True) + epsilon)
             normed = head_out * scale * gain("g_heads")[:, cols]
             mixed_all[p, kv, :, cols] = (normed * silu(out_gate)).astype(bf16)
-        sent_mixed.append(gather(mixed_all.at[p], "kv"))
+        sent_mixed.append(spread_start(mixed_all.at[p], False, p, 0))
+        if p + 1 < parts:
+            sum_merge(sent_a[p + 1])
+            sum_merge(sent_b[p + 1])
 
     copies["w_out"].wait()
-    sent_attn = []
+    by_chip = n_tp % 2 == 0
+    chip = tp // 2
+    chips = n_tp // 2
+    mine = chips + lax.rem(tp, 2)
+    other = chips + 1 - lax.rem(tp, 2)
+    beside = tp + 1 - 2 * lax.rem(tp, 2)
+
+    def chip_sum(p, condition):
+        there, here = attn_all.at[p, mine], attn_all.at[p, chip]
+        sent, received = tp_sems(p)
+
+        def add():
+            arrived(attn_all.at[p, other], received)
+            both = attn_all[p, mine].astype(f32) + attn_all[p, other].astype(f32)
+            attn_all[p, chip] = both.astype(bf16)
+            for o in range(1, chips):
+                target = lax.rem(tp + 2 * o, n_tp)
+                described(here, here, "tp", target, sent, received + 1).start()
+
+        when(condition, add)
+
+    def chip_wait(p):
+        if chips > 1:
+            arrived(attn_all.at[p, 0 : chips - 1], tp_sems(p)[1] + 1)
+
     for p in range(parts):
-        wait_all(sent_mixed[p])
+        spread_wait(sent_mixed[p])
         part = jnp.dot(joined(mixed_all[p]), vm["w_out"][...], preferred_element_type=f32)
-        attn_all[p, tp] = part.astype(bf16)
-        sent_attn.append(gather_tp(attn_all.at[p]))
+        attn_all[p, mine if by_chip else tp] = part.astype(bf16)
+        if by_chip:
+            there = attn_all.at[p, mine]
+            sent, received = tp_sems(p)
+            described(there, there, "tp", beside, sent, received).start()
+            chip_sum(p, single)
+        else:
+            gather_tp(attn_all.at[p], p)
+    if by_chip:
+        for p in range(parts):
+            chip_sum(p, paired)
+    drain()
 
     copies["g_ffn"].wait()
     copies["w_gate"].wait()
@@ -464,9 +477,13 @@
     middles = []
     sent_gu = []
     for p in range(parts):
-        wait_all(sent_attn[p])
+        if by_chip:
+            chip_wait(p)
+            drain_later(None, attn_all.at[p, 0:chips], tp_sems(p)[0])
+        else:
+            gather_wait(attn_all.at[p], p)
         attention = attn_all[p, 0].astype(f32)
-        for t in range(1, n_tp):
+        for t in range(1, chips if by_chip else n_tp):
             attention = attention + attn_all[p, t].astype(f32)
         middle = (rows_of(inputs, p) + attention).astype(bf16).astype(f32)
         normed_mid = (middle * gain("g_ffn")).astype(bf16)
@@ -480,7 +497,8 @@
                 part = jnp.dot(normed_mid, vm[name][:, lo:hi], preferred_element_type=f32)
                 store_rows(gu_send[c], p, index * (hi - lo), part.astype(bf16))
             refs = (gu_send[c].at[p], gu_recv[c].at[p], gu_merge[c].at[p])
-            sent_gu[p].append(sum_start(*refs, p in MERGE_GU))
+            sent_gu[p].append(sum_start(*refs, p in MERGE_GU, p, c))
+    gate_drains = len(drains)
     order = [(p, c) for p in range(parts) for c in range(len(bounds))]
     ahead = order[len(bounds) :]
     for c in range(len(bounds)):
@@ -497,7 +515,7 @@
         gate = reduced(gu_send[c], gu_recv[c], p, 0, w) * mid_inverse
         up = reduced(gu_send[c], gu_recv[c], p, w, 2 * w) * mid_inverse
         hid_all[c][p, kv] = (silu(gate) * up).astype(bf16)
-        sent_hid[p].append(spread_start(hid_all[c].at[p], p in RELAY))
+        sent_hid[p].append(spread_start(hid_all[c].at[p], p in RELAY, p, c))
         passing.append(sent_hid[p][c])
         if ahead:
             q, e = ahead.pop(0)
@@ -505,7 +523,10 @@
         elif len(passing) > 1:
             spread_pass(passing.pop(0))
     copies["w_down"].wait()
-    sent_down = []
+    held = drains[:]
+    drains.clear()
+    for condition, copy in held[:gate_drains]:
+        when(condition, copy.wait_send)
     for p in range(parts):
         if p == parts - 1:
             for started in passing:
@@ -516,18 +537,19 @@
             part = jnp.dot(joined(hid_all[c][p]), vm["w_down"][lo:hi], preferred_element_type=f32)
             down = part if down is None else down + part
         down_all[p, tp] = down.astype(bf16)
-        sent_down.append(gather_tp(down_all.at[p]))
+        gather_tp(down_all.at[p], p)
+    for condition, copy in held[gate_drains:]:
+        when(condition, copy.wait_send)
     finals = []
     for p in range(parts):
-        wait_all(sent_down[p])
+        gather_wait(down_all.at[p], p)
         total = down_all[p, 0].astype(f32)
         for t in range(1, n_tp):
             total = total + down_all[p, t].astype(f32)
         finals.append(middles[p] + total)
     ordered = [finals[p][d * sub : (d + 1) * sub] for d in range(n_kv) for p in range(parts)]
     out_ref[...] = jnp.concatenate(ordered, axis=0).astype(bf16)
-    for condition, copy in sends:
-        when(condition, copy.wait_send)
+    drain()
 
 
 ORDER = (
@@ -553,11 +575,13 @@
 CHUNKS = 2
 PARTS = 2
 HOLD = 0
+LATER = 0
 RELAY = (0,)
-MERGE_A = (0, 1)
-MERGE_B = (0, 1)
+MERGE_A = (1,)
+MERGE_B = (1,)
 MERGE_GU = (0, 1)
 EARLY = 7
+FIRST = 5
 
 
 def body(n_kv, n_tp, lengths, given):
@@ -574,9 +598,8 @@
     out_cols = given["w_out"].shape[1]
     parts = PARTS if seqs % (8 * PARTS) == 0 else 1
     sub = seqs // parts
-    each = max(n_kv - 1, 5)
-    remote_count = parts * (each * (3 + 2 * chunks) + 2 * (n_tp - 1))
-    scratch = [pltpu.VMEM(given[name].shape, given[name].dtype) for name in ORDER]
+    scratch = [pltpu.SMEM(lengths.shape, lengths.dtype)]
+    scratch += [pltpu.VMEM(given[name].shape, given[name].dtype) for name in ORDER]
     scratch += [
         pltpu.VMEM((seqs, kw), f32),
         pltpu.VMEM((seqs, heads, dk, dv), bf16),
@@ -591,27 +614,26 @@
         pltpu.VMEM((parts, 2, sub, 3 * kw + LANES), bf16),
         pltpu.VMEM((parts, 2, sub, 2 * vw), bf16),
         pltpu.VMEM((parts, n_kv, sub, vw), bf16),
-        pltpu.VMEM((parts, n_tp, n_kv * sub, out_cols), bf16),
+        pltpu.VMEM((parts, max(n_tp, n_tp // 2 + 2), n_kv * sub, out_cols), bf16),
         [pltpu.VMEM((parts, n_kv, sub, w), bf16) for w in gu_widths],
         [pltpu.VMEM((parts, n_kv - 1, sub, w), bf16) for w in gu_widths],
         [pltpu.VMEM((parts, 2, sub, w), bf16) for w in gu_widths],
         [pltpu.VMEM((parts, n_kv, sub, w), bf16) for w in widths],
         pltpu.VMEM((parts, n_tp, n_kv * sub, out_cols), bf16),
-        pltpu.SemaphoreType.DMA((len(ORDER),)),
-        pltpu.SemaphoreType.DMA((remote_count,)),
-        pltpu.SemaphoreType.DMA((remote_count,)),
+        pltpu.SemaphoreType.DMA((len(ORDER) + 1 - FIRST,)),
+        pltpu.SemaphoreType.DMA((parts * (max(2, chunks) + chunks + 1),)),
+        pltpu.SemaphoreType.DMA((parts * (3 * max(2, chunks) + 2 * chunks + 3),)),
     ]
     cfg = (n_kv, n_tp, ORDER, bounds, parts)
     return pl.pallas_call(
         functools.partial(kernel, cfg),
         out_shape=pltpu.VMEM((rows, columns), bf16),
-        in_specs=[pl.BlockSpec(memory_space=pltpu.SMEM)]
-        + [pl.BlockSpec(memory_space=pltpu.HBM)] * len(ORDER),
+        in_specs=[pl.BlockSpec(memory_space=pltpu.HBM)] * (len(ORDER) + 1),
         out_specs=pl.BlockSpec(memory_space=pltpu.VMEM),
         scratch_shapes=scratch,
         compiler_params=pltpu.CompilerParams(collective_id=0, has_side_effects=True),
         name="layer",
-    )(lengths, *[given[name] for name in ORDER])
+    )(*[given[name] for name in ORDER], lengths)
 
 
 NAMES = (

time: 37.7 us -> 35.6 us (0.944)
  Pallas kernels: 36.9 us -> 34.8 us
    pallas_call x1, Pallas kernels: 36.9 us -> 34.8 us  [body(): pl.pallas_call(functools.partial(kernel, cfg), out_shape=pltpu.VMEM((rows...]
where the time goes in v3:
time: 35.6 us; the launch traced here: 35.5 us
  Pallas kernels  34.8 us (98%)
  local copies, waits for them, and re-layouts  0.63 us (2%)
    pallas_call x1, Pallas kernels, body(): pl.pallas_call(functools.partial(kernel, cfg), out_shape=pltpu.VMEM((rows...  34.8 us

profile of v3, /device:TPU:0, one launch (start us, length us, event | category | flops | bytes accessed | tf_op | source)
XLA Modules:
  0.0 35.5 jit_solution(11872660663978651296)
XLA Ops:
  0.0 34.8 %layer.1 = bf16[64,512]{1,0:T(8,128)(2,1)S(1)} custom-call(bf16[64,512]{1,0:T(8,128)(2,1)} %refs_0_.1, bf16[512]{0:T(512)(128)(2,1)} %refs_1_.1, bf16[512,256]{1,0:T(8,128)(2,1)} %refs_2_.1, bf16[512,256]{1,0:T(8,128)(2,1)} %refs_3_.1, bf16[512,256]{1,0:T(8,128)(2,1)} %refs_4_.1, bf16[512,512]{1,0:T(8,128)(2,1)} %refs_5_.1, bf16[512,512]{1,0:T(8,128)(2,1)} %refs_6_.1, ...), custom_call_target="tpu_custom_call" | custom-call | tf_op jit(solution)/shard_map/layer/pallas_call | solution.py:628
  34.8 0.6 %copy.21 = bf16[64,512]{1,0:T(8,128)(2,1)} copy(bf16[64,512]{1,0:T(8,128)(2,1)S(1)} %layer.1) | data formatting | bytes 131072

commit v4 on v3

--- a/solution.py
+++ b/solution.py
@@ -154,14 +154,19 @@
             when(condition, copy.wait_send)
         drains.clear()
 
-    def sum_start(send, recv, merge, merged, p, k):
+    def targets():
+        if line and FAR:
+            return (far_outer, far_inner, partner)
+        return tuple(lax.rem(kv + o, n_kv) for o in far_first(n_kv))
+
+    def sum_start(send, recv, merge, merged, p, k, who=None):
         sent, received = sum_sems(p, k)
         merged = merged and line
 
         def direct():
-            for o in far_first(n_kv):
-                target = lax.rem(kv + o, n_kv)
-                described(send.at[target], recv.at[o - 1], "kv", target, sent, received).start()
+            for target in targets():
+                slot = lax.rem(target - kv + n_kv, n_kv) - 1
+                described(send.at[target], recv.at[slot], "kv", target, sent, received).start()
 
         def to_pair(block, ref, sem):
             described(send.at[block], ref, "kv", partner, sent, sem).start()
@@ -171,12 +176,15 @@
             to_pair(far_inner, merge.at[1], received + 2)
 
         if merged:
-            when(paired_outer, halves)
-            when(paired, lambda: to_pair(partner, recv.at[0], received))
-            when(single, direct)
+            if who is not single:
+                when(paired_outer, halves)
+                when(paired, lambda: to_pair(partner, recv.at[0], received))
+            if who is not paired:
+                when(single, direct)
         else:
-            direct()
-        drain_later(None, recv, sent)
+            when(who, direct)
+        if who is not single:
+            drain_later(None, recv, sent)
         return (send, recv, merge, merged, sent, received)
 
     def sum_merge(started):
@@ -208,8 +216,8 @@
             described(buffer.at[kv], buffer.at[kv], "kv", target, sent, sem).start()
 
         def direct():
-            for o in far_first(n_kv):
-                own(lax.rem(kv + o, n_kv), received)
+            for target in targets():
+                own(target, received)
 
         def short():
             own(far_inner, received + 1)
@@ -302,39 +310,32 @@
     inputs = vm["tokens"][...].astype(f32)
     scaled = (inputs * gain("g_mix")).astype(bf16)
     store_all(a_send, 3 * kw, split_hi_lo(jnp.sum(inputs * inputs, axis=1, keepdims=True)))
+    for name in ("w_query", "w_key", "w_decay"):
+        copies[name].wait()
     for index, name in enumerate(("w_query", "w_key", "w_decay")):
-        copies[name].wait()
         part = jnp.dot(scaled, vm[name][...], preferred_element_type=f32)
         store_all(a_send, index * kw, part.astype(bf16))
     for name in names[EARLY:]:
         copies[name].start()
     copies["lengths"].start()
     pl.semaphore_wait(barrier, n_kv - 1 + n_tp - 1)
-    if line and HOLD:
-
-        @pl.when(paired)
-        def _():
-            pl.delay(HOLD)
-
-    def start_a(p):
-        return sum_start(a_send.at[p], a_recv.at[p], a_merge.at[p], p in MERGE_A, p, 0)
-
-    def start_b(p):
-        return sum_start(b_send.at[p], b_recv.at[p], b_merge.at[p], p in MERGE_B, p, 1)
+    def start_a(p, who=None):
+        return sum_start(a_send.at[p], a_recv.at[p], a_merge.at[p], p in MERGE_A, p, 0, who)
+
+    def start_b(p, who=None):
+        return sum_start(b_send.at[p], b_recv.at[p], b_merge.at[p], p in MERGE_B, p, 1, who)
 
     sent_a = [start_a(0)]
+    for name in ("w_value", "w_outgate"):
+        copies[name].wait()
     for index, name in enumerate(("w_value", "w_outgate")):
-        copies[name].wait()
         part = jnp.dot(scaled, vm[name][...], preferred_element_type=f32)
         store_all(b_send, index * vw, part.astype(bf16))
-    sent_b = [start_b(0)]
-    def start_later():
-        for p in range(1, parts):
-            sent_a.append(start_a(p))
-            sent_b.append(start_b(p))
-
-    if LATER == 0:
-        start_later()
+    first = single if line and YIELD else None
+    sent_b = [start_b(0, first if YIELD == 2 else None)]
+    for p in range(1, parts):
+        sent_a.append(start_a(p, first))
+        sent_b.append(start_b(p, first))
 
     copies["cum_decay"].wait()
     copies["state"].wait()
@@ -357,8 +358,12 @@
         return carry
 
     lax.fori_loop(0, seqs // group, prepare, 0)
-    if LATER == 1:
-        start_later()
+    if line and YIELD:
+        if YIELD == 2:
+            start_b(0, paired)
+        for p in range(1, parts):
+            start_a(p, paired)
+            start_b(p, paired)
     for name in ("step_decay", "key_block", "value_block", "g_heads"):
         copies[name].wait()
 
@@ -398,9 +403,6 @@
     for p in range(parts):
         own_rows = slice(p * sub, (p + 1) * sub)
         sum_wait(sent_a[p])
-        if p == 0:
-            if LATER == 2:
-                start_later()
         square = join_hi_lo(reduced(a_send, a_recv, p, 3 * kw, 3 * kw + LANES))
         inverse = lax.rsqrt(square / width + epsilon)
         query = reduced(a_send, a_recv, p, 0, kw) * inverse * dk ** (-0.5)
@@ -572,10 +574,10 @@
     "w_up",
     "w_down",
 )
-CHUNKS = 2
+CHUNKS = 3
 PARTS = 2
-HOLD = 0
-LATER = 0
+YIELD = 0
+FAR = True
 RELAY = (0,)
 MERGE_A = (1,)
 MERGE_B = (1,)

time: 35.6 us -> 34.7 us (0.975)
  Pallas kernels: 34.8 us -> 33.9 us
    pallas_call x1, Pallas kernels: 34.8 us -> 33.9 us  [body(): pl.pallas_call(functools.partial(kernel, cfg), out_shape=pltpu.VMEM((rows...]
where the time goes in v4:
time: 34.7 us; the launch traced here: 34.6 us
  Pallas kernels  33.9 us (98%)
  local copies, waits for them, and re-layouts  0.63 us (2%)
    pallas_call x1, Pallas kernels, body(): pl.pallas_call(functools.partial(kernel, cfg), out_shape=pltpu.VMEM((rows...  33.9 us

profile of v4, /device:TPU:0, one launch (start us, length us, event | category | flops | bytes accessed | tf_op | source)
XLA Modules:
  0.0 34.6 jit_solution(7893528441639150692)
XLA Ops:
  0.0 33.9 %layer.1 = bf16[64,512]{1,0:T(8,128)(2,1)S(1)} custom-call(bf16[64,512]{1,0:T(8,128)(2,1)} %refs_0_.1, bf16[512]{0:T(512)(128)(2,1)} %refs_1_.1, bf16[512,256]{1,0:T(8,128)(2,1)} %refs_2_.1, bf16[512,256]{1,0:T(8,128)(2,1)} %refs_3_.1, bf16[512,256]{1,0:T(8,128)(2,1)} %refs_4_.1, bf16[512,512]{1,0:T(8,128)(2,1)} %refs_5_.1, bf16[512,512]{1,0:T(8,128)(2,1)} %refs_6_.1, ...), custom_call_target="tpu_custom_call" | custom-call | tf_op jit(solution)/shard_map/layer/pallas_call | solution.py:630
  33.9 0.6 %copy.21 = bf16[64,512]{1,0:T(8,128)(2,1)} copy(bf16[64,512]{1,0:T(8,128)(2,1)S(1)} %layer.1) | data formatting | bytes 131072

commit v5 on v4

--- a/solution.py
+++ b/solution.py
@@ -91,25 +91,29 @@
 
     copies = {}
     for index, name in enumerate(names):
-        reused = EARLY <= index < EARLY + FIRST
-        sem = index if index < EARLY else index - (EARLY if reused else FIRST)
+        if index >= LAST:
+            sem = index - LAST
+        elif index >= EARLY + FIRST:
+            sem = index - FIRST
+        else:
+            sem = index % EARLY
         copies[name] = pltpu.make_async_copy(hbm[name], vm[name], local_sem.at[sem])
     for name in names[:EARLY]:
         copies[name].start()
-    copies["lengths"] = pltpu.make_async_copy(lengths_hbm, lengths, local_sem.at[count - FIRST])
+    copies["lengths"] = pltpu.make_async_copy(lengths_hbm, lengths, local_sem.at[LAST - FIRST])
 
     def gain(name):
         return vm[name][...].astype(f32).reshape(1, -1)
 
     steps = max(2, len(bounds))
-    per_recv = 3 * steps + 2 * len(bounds) + 3
+    per_recv = 3 * steps + len(bounds) + 3
     per_send = steps + len(bounds) + 1
 
     def sum_sems(p, k):
         return (p * per_send + k, p * per_recv + 3 * k)
 
     def spread_sems(p, c):
-        return (p * per_send + steps + c, p * per_recv + 3 * steps + 2 * c)
+        return (p * per_send + steps + c, p * per_recv + 3 * steps + c)
 
     def tp_sems(p):
         return (p * per_send + steps + len(bounds), (p + 1) * per_recv - 3)
@@ -211,6 +215,7 @@
     def spread_start(buffer, relayed, p, c):
         sent, received = spread_sems(p, c)
         relayed = relayed and line
+        passed = parts * per_recv + p * len(bounds) + c
 
         def own(target, sem):
             described(buffer.at[kv], buffer.at[kv], "kv", target, sent, sem).start()
@@ -220,7 +225,7 @@
                 own(target, received)
 
         def short():
-            own(far_inner, received + 1)
+            own(far_inner, passed)
             own(partner, received)
 
         if relayed:
@@ -232,25 +237,25 @@
         else:
             direct()
             drain_later(None, buffer.at[0 : n_kv - 1], sent)
-        return (buffer, relayed, sent, received)
+        return (buffer, relayed, sent, received, passed)
 
     def spread_pass(started):
-        buffer, relayed, sent, received = started
+        buffer, relayed, sent, received, passed = started
 
         def both():
-            arrived(buffer.at[0:2], received + 1)
+            arrived(buffer.at[0:2], passed)
             for owner in (far_inner, far_outer):
                 block = buffer.at[owner]
-                described(block, block, "kv", partner, sent, received + 1).start()
+                described(block, block, "kv", partner, sent, passed).start()
 
         if relayed:
             when(paired_inner, both)
 
     def spread_wait(started):
-        buffer, relayed, sent, received = started
+        buffer, relayed, sent, received, passed = started
         if relayed:
             when(paired, lambda: arrived(buffer.at[0], received))
-            when(paired_outer, lambda: arrived(buffer.at[0:2], received + 1))
+            when(paired_outer, lambda: arrived(buffer.at[0:2], passed))
             when(single, lambda: arrived(buffer.at[0 : n_kv - 1], received))
         else:
             arrived(buffer.at[0 : n_kv - 1], received)
@@ -315,7 +320,7 @@
     for index, name in enumerate(("w_query", "w_key", "w_decay")):
         part = jnp.dot(scaled, vm[name][...], preferred_element_type=f32)
         store_all(a_send, index * kw, part.astype(bf16))
-    for name in names[EARLY:]:
+    for name in names[EARLY:LAST]:
         copies[name].start()
     copies["lengths"].start()
     pl.semaphore_wait(barrier, n_kv - 1 + n_tp - 1)
@@ -366,6 +371,8 @@
             start_b(p, paired)
     for name in ("step_decay", "key_block", "value_block", "g_heads"):
         copies[name].wait()
+    for name in names[LAST:]:
+        copies[name].start()
 
     live_ordinal = lax.broadcasted_iota(jnp.int32, (block_len, 1), 0)
 
@@ -502,9 +509,10 @@
             sent_gu[p].append(sum_start(*refs, p in MERGE_GU, p, c))
     gate_drains = len(drains)
     order = [(p, c) for p in range(parts) for c in range(len(bounds))]
-    ahead = order[len(bounds) :]
-    for c in range(len(bounds)):
-        sum_merge(sent_gu[0][c])
+    start = min(len(order), len(bounds) + AHEAD)
+    ahead = order[start:]
+    for p, c in order[:start]:
+        sum_merge(sent_gu[p][c])
     sent_hid = [[] for _ in range(parts)]
     passing = []
     for p, c in order:
@@ -574,7 +582,8 @@
     "w_up",
     "w_down",
 )
-CHUNKS = 3
+SHARES = (3, 5, 3)
+AHEAD = 1
 PARTS = 2
 YIELD = 0
 FAR = True
@@ -584,6 +593,7 @@
 MERGE_GU = (0, 1)
 EARLY = 7
 FIRST = 5
+LAST = 13
 
 
 def body(n_kv, n_tp, lengths, given):
@@ -592,8 +602,9 @@
     kw, vw = heads * dk, heads * dv
     hidden = given["w_gate"].shape[1]
     tiles = -(-hidden // LANES)
-    chunks = min(CHUNKS, tiles)
-    edges = [min(-(-tiles * c // chunks) * LANES, hidden) for c in range(chunks + 1)]
+    ends = [sum(SHARES[:c]) for c in range(len(SHARES) + 1)]
+    edges = sorted({min(-(-tiles * end // ends[-1]) * LANES, hidden) for end in ends})
+    chunks = len(edges) - 1
     bounds = tuple(zip(edges[:-1], edges[1:]))
     widths = [hi - lo for lo, hi in bounds]
     gu_widths = [2 * w + (LANES if c == 0 else 0) for c, w in enumerate(widths)]
@@ -622,9 +633,9 @@
         [pltpu.VMEM((parts, 2, sub, w), bf16) for w in gu_widths],
         [pltpu.VMEM((parts, n_kv, sub, w), bf16) for w in widths],
         pltpu.VMEM((parts, n_tp, n_kv * sub, out_cols), bf16),
-        pltpu.SemaphoreType.DMA((len(ORDER) + 1 - FIRST,)),
+        pltpu.SemaphoreType.DMA((LAST + 1 - FIRST,)),
         pltpu.SemaphoreType.DMA((parts * (max(2, chunks) + chunks + 1),)),
-        pltpu.SemaphoreType.DMA((parts * (3 * max(2, chunks) + 2 * chunks + 3),)),
+        pltpu.SemaphoreType.DMA((parts * (3 * max(2, chunks) + chunks + 3) + len(RELAY) * chunks,)),
     ]
     cfg = (n_kv, n_tp, ORDER, bounds, parts)
     return pl.pallas_call(

time: 34.7 us -> 34.5 us (level)
  no operation moved by 1% of the time
where the time goes in v5:
time: 34.5 us; the launch traced here: 34.3 us
  Pallas kernels  33.7 us (98%)
  local copies, waits for them, and re-layouts  0.63 us (2%)
    pallas_call x1, Pallas kernels, body(): pl.pallas_call(functools.partial(kernel, cfg), out_shape=pltpu.VMEM((rows...  33.7 us

profile of v5, /device:TPU:0, one launch (start us, length us, event | category | flops | bytes accessed | tf_op | source)
XLA Modules:
  0.0 34.3 jit_solution(11116293493297774331)
XLA Ops:
  0.0 33.7 %layer.1 = bf16[64,512]{1,0:T(8,128)(2,1)S(1)} custom-call(bf16[64,512]{1,0:T(8,128)(2,1)} %refs_0_.1, bf16[512]{0:T(512)(128)(2,1)} %refs_1_.1, bf16[512,256]{1,0:T(8,128)(2,1)} %refs_2_.1, bf16[512,256]{1,0:T(8,128)(2,1)} %refs_3_.1, bf16[512,256]{1,0:T(8,128)(2,1)} %refs_4_.1, bf16[512,512]{1,0:T(8,128)(2,1)} %refs_5_.1, bf16[512,512]{1,0:T(8,128)(2,1)} %refs_6_.1, ...), custom_call_target="tpu_custom_call" | custom-call | tf_op jit(solution)/shard_map/layer/pallas_call | solution.py:641
  33.7 0.6 %copy.21 = bf16[64,512]{1,0:T(8,128)(2,1)} copy(bf16[64,512]{1,0:T(8,128)(2,1)S(1)} %layer.1) | data formatting | bytes 131072

commit v6 on v5

--- a/solution.py
+++ b/solution.py
@@ -314,10 +314,10 @@
     copies["g_mix"].wait()
     inputs = vm["tokens"][...].astype(f32)
     scaled = (inputs * gain("g_mix")).astype(bf16)
-    store_all(a_send, 3 * kw, split_hi_lo(jnp.sum(inputs * inputs, axis=1, keepdims=True)))
+    store_all(a_send, 2 * kw, split_hi_lo(jnp.sum(inputs * inputs, axis=1, keepdims=True)))
     for name in ("w_query", "w_key", "w_decay"):
         copies[name].wait()
-    for index, name in enumerate(("w_query", "w_key", "w_decay")):
+    for index, name in enumerate(("w_query", "w_decay")):
         part = jnp.dot(scaled, vm[name][...], preferred_element_type=f32)
         store_all(a_send, index * kw, part.astype(bf16))
     for name in names[EARLY:LAST]:
@@ -336,6 +336,8 @@
     for index, name in enumerate(("w_value", "w_outgate")):
         part = jnp.dot(scaled, vm[name][...], preferred_element_type=f32)
         store_all(b_send, index * vw, part.astype(bf16))
+    part = jnp.dot(scaled, vm["w_key"][...], preferred_element_type=f32)
+    store_all(b_send, 2 * vw, part.astype(bf16))
     first = single if line and YIELD else None
     sent_b = [start_b(0, first if YIELD == 2 else None)]
     for p in range(1, parts):
@@ -410,11 +412,10 @@
     for p in range(parts):
         own_rows = slice(p * sub, (p + 1) * sub)
         sum_wait(sent_a[p])
-        square = join_hi_lo(reduced(a_send, a_recv, p, 3 * kw, 3 * kw + LANES))
+        square = join_hi_lo(reduced(a_send, a_recv, p, 2 * kw, 2 * kw + LANES))
         inverse = lax.rsqrt(square / width + epsilon)
         query = reduced(a_send, a_recv, p, 0, kw) * inverse * dk ** (-0.5)
-        keys_new = reduced(a_send, a_recv, p, kw, 2 * kw) * inverse
-        decay_pre = reduced(a_send, a_recv, p, 2 * kw, 3 * kw) * inverse
+        decay_pre = reduced(a_send, a_recv, p, kw, 2 * kw) * inverse
         log_sigmoid = jnp.minimum(decay_pre, 0.0) - jnp.log(1.0 + jnp.exp(-jnp.abs(decay_pre)))
         log_step = log_sigmoid / temper + vm["step_decay"][own_rows]
         token_decay = td_base[own_rows] + log_step
@@ -423,6 +424,7 @@
         qe_ref[own_rows] = query * jnp.exp(token_decay)
         lax.fori_loop(p * sub // group, (p + 1) * sub // group, attend, 0)
         sum_wait(sent_b[p])
+        keys_new = reduced(b_send, b_recv, p, 2 * vw, 2 * vw + kw) * inverse
         for h in range(heads):
             cols = slice(h * dv, (h + 1) * dv)
             keys = slice(h * dk, (h + 1) * dk)
@@ -620,12 +622,12 @@
         pltpu.VMEM((seqs, kw), f32),
         pltpu.VMEM((seqs, kw), f32),
         pltpu.VMEM((seqs, vw), f32),
-        pltpu.VMEM((parts, n_kv, sub, 3 * kw + LANES), bf16),
-        pltpu.VMEM((parts, n_kv - 1, sub, 3 * kw + LANES), bf16),
-        pltpu.VMEM((parts, n_kv, sub, 2 * vw), bf16),
-        pltpu.VMEM((parts, n_kv - 1, sub, 2 * vw), bf16),
-        pltpu.VMEM((parts, 2, sub, 3 * kw + LANES), bf16),
-        pltpu.VMEM((parts, 2, sub, 2 * vw), bf16),
+        pltpu.VMEM((parts, n_kv, sub, 2 * kw + LANES), bf16),
+        pltpu.VMEM((parts, n_kv - 1, sub, 2 * kw + LANES), bf16),
+        pltpu.VMEM((parts, n_kv, sub, 2 * vw + kw), bf16),
+        pltpu.VMEM((parts, n_kv - 1, sub, 2 * vw + kw), bf16),
+        pltpu.VMEM((parts, 2, sub, 2 * kw + LANES), bf16),
+        pltpu.VMEM((parts, 2, sub, 2 * vw + kw), bf16),
         pltpu.VMEM((parts, n_kv, sub, vw), bf16),
         pltpu.VMEM((parts, max(n_tp, n_tp // 2 + 2), n_kv * sub, out_cols), bf16),
         [pltpu.VMEM((parts, n_kv, sub, w), bf16) for w in gu_widths],

time: 34.5 us -> 34.5 us (level)
  no operation moved by 1% of the time
where the time goes in v6:
time: 34.5 us; the launch traced here: 34.4 us
  Pallas kernels  33.7 us (98%)
  local copies, waits for them, and re-layouts  0.63 us (2%)
    pallas_call x1, Pallas kernels, body(): pl.pallas_call(functools.partial(kernel, cfg), out_shape=pltpu.VMEM((rows...  33.7 us

profile of v6, /device:TPU:0, one launch (start us, length us, event | category | flops | bytes accessed | tf_op | source)
XLA Modules:
  0.0 34.4 jit_solution(16668029794856730007)
XLA Ops:
  0.0 33.7 %layer.1 = bf16[64,512]{1,0:T(8,128)(2,1)S(1)} custom-call(bf16[64,512]{1,0:T(8,128)(2,1)} %refs_0_.1, bf16[512]{0:T(512)(128)(2,1)} %refs_1_.1, bf16[512,256]{1,0:T(8,128)(2,1)} %refs_2_.1, bf16[512,256]{1,0:T(8,128)(2,1)} %refs_3_.1, bf16[512,256]{1,0:T(8,128)(2,1)} %refs_4_.1, bf16[512,512]{1,0:T(8,128)(2,1)} %refs_5_.1, bf16[512,512]{1,0:T(8,128)(2,1)} %refs_6_.1, ...), custom_call_target="tpu_custom_call" | custom-call | tf_op jit(solution)/shard_map/layer/pallas_call | solution.py:643
  33.7 0.6 %copy.21 = bf16[64,512]{1,0:T(8,128)(2,1)} copy(bf16[64,512]{1,0:T(8,128)(2,1)S(1)} %layer.1) | data formatting | bytes 131072
